TPU v7x, 128 devices: a whole 4x4x4 slice. The times are simulated.
128 devices in a mesh: sp: 16 (over z, y), tp: 8 (over x, core).
Axes of the slice: x: 4, y: 4, z: 4, core: 2. Of those that a mesh axis runs over, the one named last changes fastest.
Arguments:
- target: bfloat16 [4096, 2048], P(('sp', 'tp')), may hold values from -6 to 6
- source: bfloat16 [8192, 2048], P(('sp', 'tp')), may hold values from -6 to 6
- target_gain: bfloat16 [2, 2048], replicated, may hold values from 0.099609375 to 1.8984375
- source_gain: bfloat16 [2, 2048], replicated, may hold values from 0.099609375 to 1.8984375
- query_w: bfloat16 [2, 2048, 8192], P(None, None, 'tp'), may hold values from -0.125 to 0.125
- key_w: bfloat16 [2, 2048, 4096], P(None, None, 'tp'), may hold values from -0.125 to 0.125
- value_w: bfloat16 [2, 2048, 4096], P(None, None, 'tp'), may hold values from -0.125 to 0.125
- out_w: bfloat16 [2, 8192, 2048], P(None, 'tp'), may hold values from -0.1875 to 0.1875
- head_temp: float32 [2, 16], P(None, 'tp'), may hold values from 1.5 to 8, as said below
- final_gain: bfloat16 [2048], replicated, may hold values from 0.099609375 to 1.8984375
Outputs:
- result: float32 [4096, 2048], P(('sp', 'tp'))
Inputs may be any that keep to these rules, and one draw needn't show every extreme that they name: `head_temp`: a positive scale for each head's scores.
All inputs are finite; a program needn't handle non-finite values.
Results may differ from a plain program's by a relative error of at most 0.04.
Values may be sent and summed in bfloat16 or wider, within the bound.
A program may use at most 192 MiB of HBM per device.

v0:
```python
import jax
import jax.numpy as jnp
from jax import lax
from jax.sharding import Mesh
from jax.sharding import PartitionSpec as P

HEAD_DIM = 512
TP = ("tp_0", "tp_1")
SP_TP = ("sp", "tp_0", "tp_1")
EPS = 1e-06
FLOOR = -1e30


def laid_out(pieces, dim):
    shape = list(pieces.shape[1:])
    shape[dim] *= pieces.shape[0]
    return jnp.moveaxis(pieces, 0, dim).reshape(shape)


def copy_for_each(shard, axis):
    copies = jnp.broadcast_to(shard, (lax.axis_size(axis), *shard.shape))
    return lax.all_to_all(copies, axis, split_axis=0, concat_axis=0, tiled=True)


def collect(shard, axis, dim):
    return laid_out(copy_for_each(shard, axis), dim)


def cut_rows(length, count):
    hop = length // count
    if hop >= 8:
        hop -= hop % 8
    return [hop * k for k in range(1, count)]


def gather_in_order(shard, axes, order):
    pieces = shard
    for k in order:
        pieces = lax.all_gather(pieces, axes[k])
    done = order[::-1]
    back = [done.index(k) for k in range(len(axes))]
    pieces = pieces.transpose(*back, *range(len(axes), pieces.ndim))
    return pieces.reshape(-1, *shard.shape)


def gather_at_once(shard, axes, dim):
    numbers = list(range(len(axes)))[::-1]
    widest = shard.shape.index(max(shard.shape[:-1] or shard.shape))
    edges = [0, *cut_rows(shard.shape[widest], len(axes)), shard.shape[widest]]
    gathered = []
    for k, (start, end) in enumerate(zip(edges, edges[1:])):
        if end > start:
            share = lax.slice_in_dim(shard, start, end, axis=widest)
            gathered.append(gather_in_order(share, axes, numbers[k:] + numbers[:k]))
    return laid_out(jnp.concatenate(gathered, axis=widest + 1), dim)


def cut_along(shard, dim, count):
    shape = shard.shape
    pieces = shard.reshape(*shape[:dim], count, shape[dim] // count, *shape[dim + 1 :])
    return jnp.moveaxis(pieces, dim, 0)


def summed_on_arrival(shard, axis, dim):
    count = lax.axis_size(axis)
    pieces = lax.all_to_all(cut_along(shard, dim, count), axis, 0, 0, tiled=True)
    return jnp.sum(pieces.astype(jnp.float32), axis=0)


def unit_rows(matrix):
    values = matrix.astype(jnp.float32)
    return values * lax.rsqrt(jnp.mean(values * values, axis=-1, keepdims=True) + EPS)


def per_device(
    target, source, target_gain, source_gain, query_w, key_w, value_w, out_w, head_temp, final_gain
):
    local_heads = query_w.shape[2] // HEAD_DIM
    local_shared = key_w.shape[2] // HEAD_DIM
    group_size = local_heads // local_shared
    shared_width = key_w.shape[2]
    source_gains = source_gain.astype(jnp.float32)
    unit_piece = unit_rows(collect(source, TP, 0))
    outputs = []
    for project_layer_index in range(2):
        project_normed = (unit_piece * source_gains[project_layer_index]).astype(jnp.bfloat16)
        outputs.append(
            jnp.dot(
                project_normed, key_w[project_layer_index], preferred_element_type=jnp.float32
            ).astype(jnp.bfloat16)
        )
        outputs.append(
            jnp.dot(
                project_normed, value_w[project_layer_index], preferred_element_type=jnp.float32
            ).astype(jnp.bfloat16)
        )
    projected = jnp.concatenate(outputs, axis=1)
    hidden_state = target.astype(jnp.float32)
    for layer_index in range(2):
        key_rows = projected[
            :, 2 * layer_index * shared_width : (2 * layer_index + 1) * shared_width
        ]
        value_rows = projected[
            :, (2 * layer_index + 1) * shared_width : (2 * layer_index + 2) * shared_width
        ]
        normed = (unit_rows(hidden_state) * target_gain[layer_index].astype(jnp.float32)).astype(
            jnp.bfloat16
        )
        queries = jnp.dot(
            gather_at_once(normed, TP, 0), query_w[layer_index], preferred_element_type=jnp.float32
        ).astype(jnp.bfloat16)
        row_count = queries.shape[0]
        query_view = queries.reshape(row_count, local_shared, group_size, HEAD_DIM)
        scales = (head_temp[layer_index] * HEAD_DIM ** (-0.5)).reshape(local_shared, group_size)
        start_max = jnp.full((row_count, local_shared, group_size), FLOOR, jnp.float32)
        row_max = start_max
        key_view = lax.all_gather(key_rows, "sp", axis=0, tiled=True).reshape(
            -1, local_shared, HEAD_DIM
        )
        value_view = lax.all_gather(value_rows, "sp", axis=0, tiled=True).reshape(
            -1, local_shared, HEAD_DIM
        )
        scores = jnp.einsum(
            "tkgd,nkd->tkgn", query_view, key_view, preferred_element_type=jnp.float32
        )
        scores = scores * scales[None, :, :, None]
        new_max = jnp.maximum(row_max, jnp.max(scores, axis=-1))
        exponent = jnp.exp(scores - new_max[..., None])
        row_total = jnp.sum(exponent, axis=-1)
        accumulated = jnp.einsum(
            "tkgn,nkd->tkgd",
            exponent.astype(jnp.bfloat16),
            value_view,
            preferred_element_type=jnp.float32,
        )
        row_max, row_total, accumulated = (new_max, row_total, accumulated)
        attended = (accumulated / row_total[..., None]).astype(jnp.bfloat16)
        flat_heads = attended.reshape(row_count, local_heads * HEAD_DIM)
        mixed = summed_on_arrival(
            jnp.dot(flat_heads, out_w[layer_index], preferred_element_type=jnp.float32).astype(
                jnp.bfloat16
            ),
            TP,
            0,
        )
        hidden_state = hidden_state + mixed
    return unit_rows(hidden_state) * final_gain.astype(jnp.float32)


def solution(mesh):
    split = Mesh(mesh.devices.reshape(mesh.shape["sp"], 4, 2), ("sp", "tp_0", "tp_1"))
    in_specs = (
        P(SP_TP, None),
        P(SP_TP, None),
        P(),
        P(),
        P(None, None, TP),
        P(None, None, TP),
        P(None, None, TP),
        P(None, TP, None),
        P(None, TP),
        P(),
    )
    out_specs = P(SP_TP, None)
    return jax.shard_map(
        per_device, mesh=split, in_specs=in_specs, out_specs=out_specs, check_vma=False
    )
```

profile of v0, /device:TPU:1, one launch (start us, length us, event | category | flops | bytes accessed | tf_op | source)
XLA Modules:
  0.0 381.8 jit_solution(2791178233135704088)
XLA Ops:
  6.5 2.6 broadcast_in_dim.2
  9.1 5.8 %all-to-all-start = ((bf16[8,64,2048]{2,1,0:T(8,128)(2,1)}), bf16[8,64,2048]{2,1,0:T(8,128)(2,1)S(1)}, u32[]{:S(2)}, u32[]{:S(2)}) async-start(bf16[8,64,2048]{2,1,0:T(8,128)(2,1)} %broadcast_in_dim.2), calls=%async_computation | async-start | bytes 4194304 | tf_op jit(solution)/shard_map/all_to_all | solution.py:22
  14.9 26.2 %all-to-all-done = bf16[8,64,2048]{2,1,0:T(8,128)(2,1)S(1)} async-done(((bf16[8,64,2048]{2,1,0:T(8,128)(2,1)}), bf16[8,64,2048]{2,1,0:T(8,128)(2,1)S(1)}, u32[]{:S(2)}, u32[]{:S(2)}) %all-to-all-start) | async-done | bytes 2097184 | tf_op jit(solution)/shard_map/all_to_all | solution.py:22
  41.6 2.1 fusion.24
  45.0 2.1 fusion.70
  47.2 4.4 %fusion.67 = bf16[512,512]{1,0:T(8,128)(2,1)} fusion(bf16[512,2048]{1,0:T(8,128)(2,1)} %bitcast.231, bf16[2,2048,512]{2,1,0:T(8,128)(2,1)} %param.16), kind=kOutput, calls=%fused_computation.63 | convolution fusion | flops 1074003968 | bytes 4718592 | tf_op jit(solution)/shard_map/dot_general | solution.py:93
  51.7 3.7 fusion.76
  55.4 3.7 fusion.73
  59.4 10.6 %all-gather.2 = bf16[64,2048]{1,0:T(8,128)(2,1)S(1)} all-gather(bf16[16,2048]{1,0:T(8,128)(2,1)S(1)} %get-tuple-element.10), channel_id=4, replica_groups=mesh['sp'=16,'tp_0'=4,'tp_1'=2] {'tp_0'}, dimensions={0}, use_global_device_ids=true | all-gather | bytes 327680 | tf_op jit(solution)/shard_map/all_gather | solution.py:39
  70.0 4.6 %all-gather.3 = bf16[8,16,2048]{2,1,0:T(8,128)(2,1)S(1)} all-gather(bf16[4,16,2048]{2,1,0:T(8,128)(2,1)S(1)} %bitcast.232), channel_id=5, replica_groups=mesh['sp'=16,'tp_0'=4,'tp_1'=2] {'tp_1'}, dimensions={0}, use_global_device_ids=true | all-gather | bytes 786432 | tf_op jit(solution)/shard_map/all_gather | solution.py:39
  74.6 1.9 all-gather
  76.5 10.5 %all-gather.1 = bf16[8,16,2048]{2,1,0:T(8,128)(2,1)S(1)} all-gather(bf16[2,16,2048]{2,1,0:T(8,128)(2,1)S(1)} %bitcast.237), channel_id=3, replica_groups=mesh['sp'=16,'tp_0'=4,'tp_1'=2] {'tp_0'}, dimensions={0}, use_global_device_ids=true | all-gather | bytes 655360 | tf_op jit(solution)/shard_map/all_gather | solution.py:39
  87.1 3.5 fusion.79
  90.6 28.3 %all-gather.15.cloned.1.call-done = bf16[8192,512]{1,0:T(8,128)(2,1)} async-done(((bf16[512,512]{1,0:T(8,128)(2,1)}), bf16[8192,512]{1,0:T(8,128)(2,1)}) %all-gather.15.cloned.1.call-update) | async-done | bytes 8388624 | tf_op jit(solution)/shard_map/all_gather | solution.py:117
  118.9 11.6 %bitcast_reduce_fusion.1 = (f32[256,2]{0,1:T(2,128)S(1)}, f32[8192,256,2]{1,0,2:T(8,128)}) fusion(f32[2]{0:T(128)S(1)} %get-tuple-element.16, bf16[32,2,8,512]{3,2,1,0:T(8,128)(2,1)S(1)} %bitcast.246, bf16[8192,512]{1,0:T(8,128)(2,1)} %all-gather.15.cloned.1.call-done), kind=kOutput, calls=%fused_computation.5 | convolution fusion | flops 4303355392 | bytes 25692168 | tf_op jit(solution)/shard_map/tkgd,nkd->tkgn/dot_general | solution.py:123
  130.5 8.9 %fusion.2 = f32[256,2]{0,1:T(2,128)S(1)} fusion(f32[8192,256,2]{1,0,2:T(8,128)} %get-tuple-element.18, f32[256,2]{0,1:T(2,128)S(1)} %broadcast_maximum_fusion.1, f32[2]{0:T(128)S(1)} %get-tuple-element.16), kind=kLoop, calls=%fused_computation.8 | loop fusion | flops 12582400 | bytes 16781320 | tf_op jit(solution)/shard_map/reduce_sum | solution.py:129
  139.4 52.2 %all-gather.13.cloned.1.call-done = bf16[8192,512]{1,0:T(8,128)(2,1)} async-done(((bf16[512,512]{1,0:T(8,128)(2,1)}), bf16[8192,512]{1,0:T(8,128)(2,1)}) %all-gather.13.cloned.1.call-update) | async-done | bytes 8388624 | tf_op jit(solution)/shard_map/all_gather | solution.py:120
  191.6 12.8 %fusion.100 = bf16[1,512,256,2]{2,1,3,0:T(8,128)(2,1)S(1)} fusion(f32[8192,256,2]{1,0,2:T(8,128)} %get-tuple-element.18, f32[256,2]{0,1:T(2,128)S(1)} %broadcast_maximum_fusion.1, f32[2]{0:T(128)S(1)} %get-tuple-element.16, bf16[8192,512]{1,0:T(8,128)(2,1)} %all-gather.13.cloned.1.call-done, f32[256,2]{0,1:T(2,128)S(1)} %fusion.2), kind=kOutput, calls=%fused_computation.72 | convolution fusion | flops 4308074496 | bytes 25694216 | tf_op jit(solution)/shard_map/tkgn,nkd->tkgd/dot_general | solution.py:130
  204.4 3.7 fusion.39
  208.1 20.0 %all_to_all.15 = bf16[8,32,2048]{2,1,0:T(8,128)(2,1)S(1)} all-to-all(bf16[8,32,2048]{2,1,0:T(8,128)(2,1)S(1)} %bitcast.236), channel_id=1, replica_groups=mesh['sp'=16,'tp_0'=4,'tp_1'=2] {'tp_0','tp_1'}, dimensions={0} | all-to-all | bytes 2097152 | tf_op jit(solution)/shard_map/all_to_all | solution.py:66
  228.6 10.6 %all-gather.6 = bf16[64,2048]{1,0:T(8,128)(2,1)S(1)} all-gather(bf16[16,2048]{1,0:T(8,128)(2,1)S(1)} %get-tuple-element.8), channel_id=8, replica_groups=mesh['sp'=16,'tp_0'=4,'tp_1'=2] {'tp_0'}, dimensions={0}, use_global_device_ids=true | all-gather | bytes 327680 | tf_op jit(solution)/shard_map/all_gather | solution.py:39
  239.1 4.5 %all-gather.7 = bf16[8,16,2048]{2,1,0:T(8,128)(2,1)S(1)} all-gather(bf16[4,16,2048]{2,1,0:T(8,128)(2,1)S(1)} %bitcast.233), channel_id=9, replica_groups=mesh['sp'=16,'tp_0'=4,'tp_1'=2] {'tp_1'}, dimensions={0}, use_global_device_ids=true | all-gather | bytes 786432 | tf_op jit(solution)/shard_map/all_gather | solution.py:39
  243.7 1.9 all-gather.4
  245.6 11.3 %all-gather.5 = bf16[8,16,2048]{2,1,0:T(8,128)(2,1)S(1)} all-gather(bf16[2,16,2048]{2,1,0:T(8,128)(2,1)S(1)} %bitcast.238), channel_id=7, replica_groups=mesh['sp'=16,'tp_0'=4,'tp_1'=2] {'tp_0'}, dimensions={0}, use_global_device_ids=true | all-gather | bytes 655360 | tf_op jit(solution)/shard_map/all_gather | solution.py:39
  258.3 6.0 %all-gather.19.cloned.1.call-done = bf16[8192,512]{1,0:T(8,128)(2,1)} async-done(((bf16[512,512]{1,0:T(8,128)(2,1)}), bf16[8192,512]{1,0:T(8,128)(2,1)}) %all-gather.19.cloned.1.call-update) | async-done | bytes 8388624 | tf_op jit(solution)/shard_map/all_gather | solution.py:117
  264.3 11.6 %bitcast_reduce_fusion = (f32[256,2]{0,1:T(2,128)S(1)}, f32[8192,256,2]{1,0,2:T(8,128)}) fusion(f32[2]{0:T(128)S(1)} %get-tuple-element.15, bf16[32,2,8,512]{3,2,1,0:T(8,128)(2,1)S(1)} %bitcast.245, bf16[8192,512]{1,0:T(8,128)(2,1)} %all-gather.19.cloned.1.call-done), kind=kOutput, calls=%fused_computation.1 | convolution fusion | flops 4303355392 | bytes 25692168 | tf_op jit(solution)/shard_map/tkgd,nkd->tkgn/dot_general | solution.py:123
  275.9 8.8 %fusion.4 = f32[256,2]{0,1:T(2,128)S(1)} fusion(f32[8192,256,2]{1,0,2:T(8,128)} %get-tuple-element.20, f32[256,2]{0,1:T(2,128)S(1)} %broadcast_maximum_fusion, f32[2]{0:T(128)S(1)} %get-tuple-element.15), kind=kLoop, calls=%fused_computation.10 | loop fusion | flops 12582400 | bytes 16781320 | tf_op jit(solution)/shard_map/reduce_sum | solution.py:129
  284.8 52.1 %all-gather.17.cloned.1.call-done = bf16[8192,512]{1,0:T(8,128)(2,1)} async-done(((bf16[512,512]{1,0:T(8,128)(2,1)}), bf16[8192,512]{1,0:T(8,128)(2,1)}) %all-gather.17.cloned.1.call-update) | async-done | bytes 8388624 | tf_op jit(solution)/shard_map/all_gather | solution.py:120
  336.8 12.8 %fusion.90 = bf16[1,512,256,2]{2,1,3,0:T(8,128)(2,1)S(1)} fusion(f32[8192,256,2]{1,0,2:T(8,128)} %get-tuple-element.20, f32[256,2]{0,1:T(2,128)S(1)} %broadcast_maximum_fusion, f32[2]{0:T(128)S(1)} %get-tuple-element.15, bf16[8192,512]{1,0:T(8,128)(2,1)} %all-gather.17.cloned.1.call-done, f32[256,2]{0,1:T(2,128)S(1)} %fusion.4), kind=kOutput, calls=%fused_computation.70 | convolution fusion | flops 4308074496 | bytes 25694216 | tf_op jit(solution)/shard_map/tkgn,nkd->tkgd/dot_general | solution.py:130
  349.6 4.4 %fusion.42 = bf16[256,2048]{1,0:T(8,128)(2,1)} fusion(bf16[256,1024]{0,1:T(8,128)(2,1)S(1)} %bitcast.248, bf16[2,1024,2048]{2,1,0:T(8,128)(2,1)} %param.17), kind=kOutput, calls=%fused_computation.46 | convolution fusion | flops 1074266112 | bytes 5767168 | tf_op jit(solution)/shard_map/dot_general | solution.py:140
  354.1 5.1 %all-to-all-start.2 = ((bf16[8,32,2048]{2,1,0:T(8,128)(2,1)}), bf16[8,32,2048]{2,1,0:T(8,128)(2,1)S(1)}, u32[]{:S(2)}, u32[]{:S(2)}) async-start(bf16[8,32,2048]{2,1,0:T(8,128)(2,1)} %bitcast.45), calls=%async_computation.2 | async-start | bytes 2097152 | tf_op jit(solution)/shard_map/all_to_all | solution.py:66
  359.2 15.0 %all-to-all-done.2 = bf16[8,32,2048]{2,1,0:T(8,128)(2,1)S(1)} async-done(((bf16[8,32,2048]{2,1,0:T(8,128)(2,1)}), bf16[8,32,2048]{2,1,0:T(8,128)(2,1)S(1)}, u32[]{:S(2)}, u32[]{:S(2)}) %all-to-all-start.2) | async-done | bytes 1048608 | tf_op jit(solution)/shard_map/all_to_all | solution.py:66
  (55 shorter events, 5.3 us)
Async XLA Ops:
  6.5 8.4 %copy-start.3 = (bf16[2,2048]{1,0:T(2,128)(2,1)S(1)}, bf16[2,2048]{1,0:T(2,128)(2,1)}, u32[]{:S(2)}) copy-start(bf16[2,2048]{1,0:T(2,128)(2,1)} %param.13) | copy-start | bytes 24580
  9.1 32.0 %all-to-all-start = ((bf16[8,64,2048]{2,1,0:T(8,128)(2,1)}), bf16[8,64,2048]{2,1,0:T(8,128)(2,1)S(1)}, u32[]{:S(2)}, u32[]{:S(2)}) async-start(bf16[8,64,2048]{2,1,0:T(8,128)(2,1)} %broadcast_in_dim.2), calls=%async_computation | async-start | bytes 4194304 | tf_op jit(solution)/shard_map/all_to_all | solution.py:22
  14.9 104.0 %all-gather.15.cloned.1.call-start = ((), (), s32[]{:S(2)}) async-start(), calls=%async_computation.4 | async-start | bytes 8912896 | tf_op jit(solution)/shard_map/all_gather | solution.py:117
  41.1 3.9 %copy-start.7 = (bf16[2,2048,512]{2,1,0:T(8,128)(2,1)S(1)}, bf16[2,2048,512]{2,1,0:T(8,128)(2,1)}, u32[]{:S(2)}) copy-start(bf16[2,2048,512]{2,1,0:T(8,128)(2,1)} %param.15) | copy-start | bytes 12582916
  43.7 1.3 copy-start.2
  47.1 4.6 %copy-start.1 = (bf16[8,64,2048]{2,1,0:T(8,128)(2,1)S(1)}, bf16[8,64,2048]{2,1,0:T(8,128)(2,1)}, u32[]{:S(2)}) copy-start(bf16[8,64,2048]{2,1,0:T(8,128)(2,1)} %get-tuple-element.6) | copy-start | bytes 6291460
  47.1 144.4 %all-gather.13.cloned.1.call-start = ((), (), s32[]{:S(2)}) async-start(), calls=%async_computation.3 | async-start | bytes 8912896 | tf_op jit(solution)/shard_map/all_gather | solution.py:120
  51.6 212.6 %all-gather.19.cloned.1.call-start = ((), (), s32[]{:S(2)}) async-start(), calls=%async_computation.6 | async-start | bytes 8912896 | tf_op jit(solution)/shard_map/all_gather | solution.py:117
  55.3 3.8 copy-start
  55.3 3.9 %copy-start.4 = (bf16[2,2048]{1,0:T(2,128)(2,1)S(1)}, bf16[2,2048]{1,0:T(2,128)(2,1)}, u32[]{:S(2)}) copy-start(bf16[2,2048]{1,0:T(2,128)(2,1)} %param.12) | copy-start | bytes 24580
  55.4 31.6 %copy-start.6 = (f32[2,2]{1,0:T(2,128)S(1)}, f32[2,2]{1,0:T(2,128)}, u32[]{:S(2)}) copy-start(f32[2,2]{1,0:T(2,128)} %param.18) | copy-start | bytes 52
  55.4 281.4 %all-gather.17.cloned.1.call-start = ((), (), s32[]{:S(2)}) async-start(), calls=%async_computation.5 | async-start | bytes 8912896 | tf_op jit(solution)/shard_map/all_gather | solution.py:120
  204.4 52.6 %slice-start = ((s8[8388608]{0:T(1024)(128)(4,1)}), s8[4194304]{0:T(1024)(128)(4,1)S(1)}, s32[]{:S(2)}) async-start(s8[8388608]{0:T(1024)(128)(4,1)} %bitcast.243), calls=%async_computation.7 | async-start | bytes 8388608
  208.1 48.9 %slice-start.1 = ((s8[8388608]{0:T(1024)(128)(4,1)}), s8[4194304]{0:T(1024)(128)(4,1)S(1)}, s32[]{:S(2)}) async-start(s8[8388608]{0:T(1024)(128)(4,1)} %bitcast.243), calls=%async_computation.8 | async-start | bytes 8388608
  349.6 9.5 %copy-start.5 = (bf16[2048]{0:T(1024)(128)(2,1)S(1)}, bf16[2048]{0:T(1024)(128)(2,1)}, u32[]{:S(2)}) copy-start(bf16[2048]{0:T(1024)(128)(2,1)} %param.19) | copy-start | bytes 12292
  354.1 20.1 %all-to-all-start.2 = ((bf16[8,32,2048]{2,1,0:T(8,128)(2,1)}), bf16[8,32,2048]{2,1,0:T(8,128)(2,1)S(1)}, u32[]{:S(2)}, u32[]{:S(2)}) async-start(bf16[8,32,2048]{2,1,0:T(8,128)(2,1)} %bitcast.45), calls=%async_computation.2 | async-start | bytes 2097152 | tf_op jit(solution)/shard_map/all_to_all | solution.py:66
Sparse Core Ops, SparseCore 0:
  47.3 71.5 all-gather.14
  121.0 70.5 all-gather.12
  193.7 70.5 all-gather.18
  266.3 70.5 all-gather.16
where the time goes:
time: 382 us
  waiting for transfers between devices  180 us (47%)
  blocking collectives  75.9 us (20%)
  matrix products  75.6 us (20%)
  other arithmetic  22.3 us (6%)
  between operations  13.3 us (3%)
  starting transfers between devices  11 us (3%)
  local copies, waits for them, and re-layouts  4.03 us (1%)
    all_gather x2, waiting for transfers between devices, per_device(): lax.all_gather(value_rows, 'sp', axis=0, tiled=True)  104 us
    all_gather x8, blocking collectives, gather_in_order(): pieces = lax.all_gather(pieces, axes[k])  55.9 us
    all_gather x2, waiting for transfers between devices, per_device(): lax.all_gather(key_rows, 'sp', axis=0, tiled=True)  34.2 us
    all_to_all x1, waiting for transfers between devices, copy_for_each(): return lax.all_to_all(copies, axis, split_axis=0, concat_axis=0, tiled=True)  26.2 us
    dot_general x2, matrix products, per_device(): jnp.einsum('tkgn,nkd->tkgd', exponent.astype(jnp.bfloat16), value_view, p...  25.6 us
    dot_general x2, matrix products, per_device(): jnp.einsum('tkgd,nkd->tkgn', query_view, key_view, preferred_element_type...  23.3 us
    all_to_all x1, blocking collectives, summed_on_arrival(): lax.all_to_all(cut_along(shard, dim, count), axis, 0, 0, tiled=True)  20 us
    reduce_sum x2, other arithmetic, per_device(): row_total = jnp.sum(exponent, axis=-1)  17.7 us
  transfers between devices with their start and end apart: 6, of which 6 were waited for; matrix products, arithmetic and copies ran while one was open for 20% of the time, Pallas kernels for 0%

commit v1 on v0

--- a/solution.py
+++ b/solution.py
@@ -117,9 +117,15 @@
         key_view = lax.all_gather(key_rows, "sp", axis=0, tiled=True).reshape(
             -1, local_shared, HEAD_DIM
         )
-        value_view = lax.all_gather(value_rows, "sp", axis=0, tiled=True).reshape(
-            -1, local_shared, HEAD_DIM
-        )
+        value_view = jnp.concatenate(
+            lax.all_to_all(
+                jnp.stack([value_rows] * lax.axis_size("sp"), 0),
+                concat_axis=0,
+                split_axis=0,
+                axis_name="sp",
+            ),
+            0,
+        ).reshape(-1, local_shared, HEAD_DIM)
         scores = jnp.einsum(
             "tkgd,nkd->tkgn", query_view, key_view, preferred_element_type=jnp.float32
         )

time: 382 us -> 509 us (1.33); the launches traced: 382 us -> 500 us
  local copies, waits for them, and re-layouts: 4.03 us -> 63 us
  waiting for transfers between devices: 180 us -> 229 us
  starting transfers between devices: 11 us -> 34.5 us
  blocking collectives: 75.9 us -> 61.7 us
    all_to_all x0 -> x2, waiting for transfers between devices: none -> 188 us  [per_device(): lax.all_to_all(jnp.stack([value_rows] * lax.axis_size('sp'), 0), concat_a...]
    all_gather x2 -> x0, waiting for transfers between devices: 104 us -> none  [per_device(): lax.all_gather(value_rows, 'sp', axis=0, tiled=True)]
    another operation x0 -> x4, local copies, waits for them, and re-layouts: none -> 35.1 us
    all_gather x2, waiting for transfers between devices: 34.2 us -> 0.02 us  [per_device(): lax.all_gather(key_rows, 'sp', axis=0, tiled=True)]
    all_to_all x0 -> x2, local copies, waits for them, and re-layouts: none -> 22.7 us  [per_device(): lax.all_to_all(jnp.stack([value_rows] * lax.axis_size('sp'), 0), concat_a...]
    all_to_all x1 -> x0, blocking collectives: 20 us -> none  [summed_on_arrival(): lax.all_to_all(cut_along(shard, dim, count), axis, 0, 0, tiled=True)]
    all_to_all x0 -> x2, starting transfers between devices: none -> 12.8 us  [per_device(): lax.all_to_all(jnp.stack([value_rows] * lax.axis_size('sp'), 0), concat_a...]
    all_to_all x1 -> x2, starting transfers between devices: 5.09 us -> 15.8 us  [summed_on_arrival(): lax.all_to_all(cut_along(shard, dim, count), axis, 0, 0, tiled=True)]
  transfers between devices with their start and end apart: 6 -> 7, of which waited for: 6 -> 4; matrix products, arithmetic and copies ran while one was open for 20% -> 23% of each run, Pallas kernels for 0% -> 0%
where the time goes in v1:
time: 509 us; the launch traced here: 500 us
  waiting for transfers between devices  229 us (45%)
  matrix products  76.9 us (15%)
  local copies, waits for them, and re-layouts  63 us (12%)
  blocking collectives  61.7 us (12%)
  starting transfers between devices  34.5 us (7%)
  other arithmetic  21.6 us (4%)
  between operations  14 us (3%)
    all_to_all x2, waiting for transfers between devices, per_device(): lax.all_to_all(jnp.stack([value_rows] * lax.axis_size('sp'), 0), concat_a...  188 us
    all_gather x8, blocking collectives, gather_in_order(): pieces = lax.all_gather(pieces, axes[k])  61.7 us
    another operation x2, local copies, waits for them, and re-layouts  27.1 us
    dot_general x2, matrix products, per_device(): jnp.einsum('tkgn,nkd->tkgd', exponent.astype(jnp.bfloat16), value_view, p...  25.7 us
    all_to_all x1, waiting for transfers between devices, copy_for_each(): return lax.all_to_all(copies, axis, split_axis=0, concat_axis=0, tiled=True)  25.4 us
    dot_general x2, matrix products, per_device(): jnp.einsum('tkgd,nkd->tkgn', query_view, key_view, preferred_element_type...  23.2 us
    all_to_all x2, local copies, waits for them, and re-layouts, per_device(): lax.all_to_all(jnp.stack([value_rows] * lax.axis_size('sp'), 0), concat_a...  22.7 us
    reduce_sum x2, other arithmetic, per_device(): row_total = jnp.sum(exponent, axis=-1)  17.1 us
  transfers between devices with their start and end apart: 7, of which 4 were waited for; matrix products, arithmetic and copies ran while one was open for 23% of the time, Pallas kernels for 0%

profile of v1, /device:TPU:1, one launch (start us, length us, event | category | flops | bytes accessed | tf_op | source)
XLA Modules:
  0.0 500.4 jit_solution(1885442664936096526)
XLA Ops:
  9.1 5.8 %all-to-all-start = ((bf16[8,64,2048]{2,1,0:T(8,128)(2,1)}), bf16[8,64,2048]{2,1,0:T(8,128)(2,1)S(1)}, u32[]{:S(2)}, u32[]{:S(2)}) async-start(bf16[8,64,2048]{2,1,0:T(8,128)(2,1)} %broadcast_in_dim.2), calls=%async_computation | async-start | bytes 4194304 | tf_op jit(solution)/shard_map/all_to_all | solution.py:22
  15.7 25.4 %all-to-all-done = bf16[8,64,2048]{2,1,0:T(8,128)(2,1)S(1)} async-done(((bf16[8,64,2048]{2,1,0:T(8,128)(2,1)}), bf16[8,64,2048]{2,1,0:T(8,128)(2,1)S(1)}, u32[]{:S(2)}, u32[]{:S(2)}) %all-to-all-start) | async-done | bytes 2097184 | tf_op jit(solution)/shard_map/all_to_all | solution.py:22
  47.1 3.5 fusion.67
  50.8 4.0 stack.4
  54.8 8.0 %all-to-all-start.1 = ((bf16[16,512,512]{1,2,0:T(8,128)(2,1)}), bf16[16,512,512]{1,2,0:T(8,128)(2,1)}, u32[]{:S(2)}, u32[]{:S(2)}) async-start(bf16[16,512,512]{1,2,0:T(8,128)(2,1)} %stack.4), calls=%async_computation.1 | async-start | bytes 16777216 | tf_op jit(solution)/shard_map/all_to_all | solution.py:121
  62.8 3.7 fusion.76
  69.8 140.1 %all-to-all-done.1 = bf16[16,512,512]{1,2,0:T(8,128)(2,1)} async-done(((bf16[16,512,512]{1,2,0:T(8,128)(2,1)}), bf16[16,512,512]{1,2,0:T(8,128)(2,1)}, u32[]{:S(2)}, u32[]{:S(2)}) %all-to-all-start.1) | async-done | bytes 8388640 | tf_op jit(solution)/shard_map/all_to_all | solution.py:121
  209.9 4.0 stack.5
  213.9 4.9 all-to-all-start.3
  218.9 15.3 %all-gather.2 = bf16[64,2048]{1,0:T(8,128)(2,1)S(1)} all-gather(bf16[16,2048]{1,0:T(8,128)(2,1)S(1)} %get-tuple-element.10), channel_id=4, replica_groups=mesh['sp'=16,'tp_0'=4,'tp_1'=2] {'tp_0'}, dimensions={0}, use_global_device_ids=true | all-gather | bytes 327680 | tf_op jit(solution)/shard_map/all_gather | solution.py:39
  234.2 5.0 all-gather.3
  241.1 11.6 %all-gather.1 = bf16[8,16,2048]{2,1,0:T(8,128)(2,1)S(1)} all-gather(bf16[2,16,2048]{2,1,0:T(8,128)(2,1)S(1)} %bitcast.224), channel_id=3, replica_groups=mesh['sp'=16,'tp_0'=4,'tp_1'=2] {'tp_0'}, dimensions={0}, use_global_device_ids=true | all-gather | bytes 655360 | tf_op jit(solution)/shard_map/all_gather | solution.py:39
  256.2 11.4 %copy.30 = bf16[16,512,512]{1,0,2:T(8,128)(2,1)} copy(bf16[16,512,512]{1,2,0:T(8,128)(2,1)} %all-to-all-done.1) | data formatting | bytes 16777216 | tf_op jit(solution)/shard_map/all_to_all | solution.py:121
  267.6 13.6 %reshape.224 = bf16[8192,512,1]{0,1,2:T(8,128)(2,1)} reshape(bf16[16,512,512]{1,0,2:T(8,128)(2,1)} %copy.30) | data formatting | bytes 16777216 | tf_op jit(solution)/shard_map/reshape.6
  281.2 11.5 %bitcast_reduce_fusion.1 = (f32[256,2]{0,1:T(2,128)S(1)}, f32[8192,256,2]{1,0,2:T(8,128)}) fusion(f32[2]{0:T(128)S(1)} %get-tuple-element.16, bf16[32,2,8,512]{3,2,1,0:T(8,128)(2,1)S(1)} %bitcast.230, bf16[8192,512]{1,0:T(8,128)(2,1)} %all-gather.11.cloned.1.call-done), kind=kOutput, calls=%fused_computation.5 | convolution fusion | flops 4303355392 | bytes 25692168 | tf_op jit(solution)/shard_map/tkgd,nkd->tkgn/dot_general | solution.py:129
  292.7 8.6 %fusion.2 = f32[256,2]{0,1:T(2,128)S(1)} fusion(f32[8192,256,2]{1,0,2:T(8,128)} %get-tuple-element.18, f32[256,2]{0,1:T(2,128)S(1)} %broadcast_maximum_fusion.1, f32[2]{0:T(128)S(1)} %get-tuple-element.16), kind=kLoop, calls=%fused_computation.8 | loop fusion | flops 12582400 | bytes 16781320 | tf_op jit(solution)/shard_map/reduce_sum | solution.py:135
  301.2 12.9 %fusion.85 = bf16[1,512,256,2]{2,1,3,0:T(8,128)(2,1)S(1)} fusion(bf16[8192,512,1]{0,1,2:T(8,128)(2,1)} %reshape.224, f32[8192,256,2]{1,0,2:T(8,128)} %get-tuple-element.18, f32[256,2]{0,1:T(2,128)S(1)} %broadcast_maximum_fusion.1, f32[2]{0:T(128)S(1)} %get-tuple-element.16, f32[256,2]{0,1:T(2,128)S(1)} %fusion.2), kind=kOutput, calls=%fused_computation.69 | convolution fusion | flops 4308074496 | bytes 25694216 | tf_op jit(solution)/shard_map/tkgn,nkd->tkgd/dot_general | solution.py:136
  314.1 4.5 fusion.37
  318.7 48.2 %all-to-all-done.3 = bf16[16,512,512]{1,2,0:T(8,128)(2,1)} async-done(((bf16[16,512,512]{1,2,0:T(8,128)(2,1)}), bf16[16,512,512]{1,2,0:T(8,128)(2,1)}, u32[]{:S(2)}, u32[]{:S(2)}) %all-to-all-start.3) | async-done | bytes 8388640 | tf_op jit(solution)/shard_map/all_to_all | solution.py:121
  366.8 9.2 %all-to-all-start.2 = ((bf16[8,32,2048]{2,1,0:T(8,128)(2,1)}), bf16[8,32,2048]{2,1,0:T(8,128)(2,1)S(1)}, u32[]{:S(2)}, u32[]{:S(2)}) async-start(bf16[8,32,2048]{2,1,0:T(8,128)(2,1)} %bitcast.21), calls=%async_computation.2 | async-start | bytes 2097152 | tf_op jit(solution)/shard_map/all_to_all | solution.py:66
  376.0 11.3 %copy.35 = bf16[16,512,512]{1,0,2:T(8,128)(2,1)} copy(bf16[16,512,512]{1,2,0:T(8,128)(2,1)} %all-to-all-done.3) | data formatting | bytes 16777216 | tf_op jit(solution)/shard_map/all_to_all | solution.py:121
  387.4 13.5 %reshape.226 = bf16[8192,512,1]{0,1,2:T(8,128)(2,1)} reshape(bf16[16,512,512]{1,0,2:T(8,128)(2,1)} %copy.35) | data formatting | bytes 16777216 | tf_op jit(solution)/shard_map/reshape.31
  401.3 10.4 %all-gather.6 = bf16[64,2048]{1,0:T(8,128)(2,1)S(1)} all-gather(bf16[16,2048]{1,0:T(8,128)(2,1)S(1)} %get-tuple-element.8), channel_id=8, replica_groups=mesh['sp'=16,'tp_0'=4,'tp_1'=2] {'tp_0'}, dimensions={0}, use_global_device_ids=true | all-gather | bytes 327680 | tf_op jit(solution)/shard_map/all_gather | solution.py:39
  411.6 4.5 all-gather.7
  418.1 11.1 %all-gather.5 = bf16[8,16,2048]{2,1,0:T(8,128)(2,1)S(1)} all-gather(bf16[2,16,2048]{2,1,0:T(8,128)(2,1)S(1)} %bitcast.225), channel_id=7, replica_groups=mesh['sp'=16,'tp_0'=4,'tp_1'=2] {'tp_0'}, dimensions={0}, use_global_device_ids=true | all-gather | bytes 655360 | tf_op jit(solution)/shard_map/all_gather | solution.py:39
  429.3 3.5 fusion.82
  432.8 11.8 %bitcast_reduce_fusion = (f32[256,2]{0,1:T(2,128)S(1)}, f32[8192,256,2]{1,0,2:T(8,128)}) fusion(f32[2]{0:T(128)S(1)} %get-tuple-element.15, bf16[32,2,8,512]{3,2,1,0:T(8,128)(2,1)S(1)} %bitcast.231, bf16[8192,512]{1,0:T(8,128)(2,1)} %all-gather.13.cloned.1.call-done), kind=kOutput, calls=%fused_computation.1 | convolution fusion | flops 4303355392 | bytes 25692168 | tf_op jit(solution)/shard_map/tkgd,nkd->tkgn/dot_general | solution.py:129
  444.6 8.6 %fusion.4 = f32[256,2]{0,1:T(2,128)S(1)} fusion(f32[8192,256,2]{1,0,2:T(8,128)} %get-tuple-element.20, f32[256,2]{0,1:T(2,128)S(1)} %broadcast_maximum_fusion, f32[2]{0:T(128)S(1)} %get-tuple-element.15), kind=kLoop, calls=%fused_computation.10 | loop fusion | flops 12582400 | bytes 16781320 | tf_op jit(solution)/shard_map/reduce_sum | solution.py:135
  453.1 12.8 %fusion.88 = bf16[1,512,256,2]{2,1,3,0:T(8,128)(2,1)S(1)} fusion(bf16[8192,512,1]{0,1,2:T(8,128)(2,1)} %reshape.226, f32[8192,256,2]{1,0,2:T(8,128)} %get-tuple-element.20, f32[256,2]{0,1:T(2,128)S(1)} %broadcast_maximum_fusion, f32[2]{0:T(128)S(1)} %get-tuple-element.15, f32[256,2]{0,1:T(2,128)S(1)} %fusion.4), kind=kOutput, calls=%fused_computation.70 | convolution fusion | flops 4308074496 | bytes 25694216 | tf_op jit(solution)/shard_map/tkgn,nkd->tkgd/dot_general | solution.py:136
  466.0 4.4 fusion.40
  470.4 6.6 %all-to-all-start.4 = ((bf16[8,32,2048]{2,1,0:T(8,128)(2,1)}), bf16[8,32,2048]{2,1,0:T(8,128)(2,1)S(1)}, u32[]{:S(2)}, u32[]{:S(2)}) async-start(bf16[8,32,2048]{2,1,0:T(8,128)(2,1)} %bitcast.43), calls=%async_computation.4 | async-start | bytes 2097152 | tf_op jit(solution)/shard_map/all_to_all | solution.py:66
  477.1 15.0 %all-to-all-done.4 = bf16[8,32,2048]{2,1,0:T(8,128)(2,1)S(1)} async-done(((bf16[8,32,2048]{2,1,0:T(8,128)(2,1)}), bf16[8,32,2048]{2,1,0:T(8,128)(2,1)S(1)}, u32[]{:S(2)}, u32[]{:S(2)}) %all-to-all-start.4) | async-done | bytes 1048608 | tf_op jit(solution)/shard_map/all_to_all | solution.py:66
  (55 shorter events, 22.0 us)
Async XLA Ops:
  9.1 32.0 %all-to-all-start = ((bf16[8,64,2048]{2,1,0:T(8,128)(2,1)}), bf16[8,64,2048]{2,1,0:T(8,128)(2,1)S(1)}, u32[]{:S(2)}, u32[]{:S(2)}) async-start(bf16[8,64,2048]{2,1,0:T(8,128)(2,1)} %broadcast_in_dim.2), calls=%async_computation | async-start | bytes 4194304 | tf_op jit(solution)/shard_map/all_to_all | solution.py:22
  14.9 266.3 %all-gather.11.cloned.1.call-start = ((), (), s32[]{:S(2)}) async-start(), calls=%async_computation.5 | async-start | bytes 8912896 | tf_op jit(solution)/shard_map/all_gather | solution.py:117
  41.1 3.9 copy-start.6
  43.7 1.3 copy-start.2
  54.8 8.0 %copy-start.1 = (bf16[8,64,2048]{2,1,0:T(8,128)(2,1)S(1)}, bf16[8,64,2048]{2,1,0:T(8,128)(2,1)}, u32[]{:S(2)}) copy-start(bf16[8,64,2048]{2,1,0:T(8,128)(2,1)} %get-tuple-element.6) | copy-start | bytes 6291460
  54.8 11.7 %copy-start = (bf16[32,2048]{1,0:T(8,128)(2,1)S(1)}, bf16[32,2048]{1,0:T(8,128)(2,1)}, u32[]{:S(2)}) copy-start(bf16[32,2048]{1,0:T(8,128)(2,1)} %param.10) | copy-start | bytes 393220
  54.8 11.9 %copy-start.3 = (bf16[2,2048]{1,0:T(2,128)(2,1)S(1)}, bf16[2,2048]{1,0:T(2,128)(2,1)}, u32[]{:S(2)}) copy-start(bf16[2,2048]{1,0:T(2,128)(2,1)} %param.12) | copy-start | bytes 24580
  54.8 155.1 %all-to-all-start.1 = ((bf16[16,512,512]{1,2,0:T(8,128)(2,1)}), bf16[16,512,512]{1,2,0:T(8,128)(2,1)}, u32[]{:S(2)}, u32[]{:S(2)}) async-start(bf16[16,512,512]{1,2,0:T(8,128)(2,1)} %stack.4), calls=%async_computation.1 | async-start | bytes 16777216 | tf_op jit(solution)/shard_map/all_to_all | solution.py:121
  62.8 370.0 %all-gather.13.cloned.1.call-start = ((), (), s32[]{:S(2)}) async-start(), calls=%async_computation.6 | async-start | bytes 8912896 | tf_op jit(solution)/shard_map/all_gather | solution.py:117
  213.9 38.8 %copy-start.5 = (f32[2,2]{1,0:T(2,128)S(1)}, f32[2,2]{1,0:T(2,128)}, u32[]{:S(2)}) copy-start(f32[2,2]{1,0:T(2,128)} %param.18) | copy-start | bytes 52
  213.9 152.9 %all-to-all-start.3 = ((bf16[16,512,512]{1,2,0:T(8,128)(2,1)}), bf16[16,512,512]{1,2,0:T(8,128)(2,1)}, u32[]{:S(2)}, u32[]{:S(2)}) async-start(bf16[16,512,512]{1,2,0:T(8,128)(2,1)} %stack.5), calls=%async_computation.3 | async-start | bytes 16777216 | tf_op jit(solution)/shard_map/all_to_all | solution.py:121
  366.8 34.0 %all-to-all-start.2 = ((bf16[8,32,2048]{2,1,0:T(8,128)(2,1)}), bf16[8,32,2048]{2,1,0:T(8,128)(2,1)S(1)}, u32[]{:S(2)}, u32[]{:S(2)}) async-start(bf16[8,32,2048]{2,1,0:T(8,128)(2,1)} %bitcast.21), calls=%async_computation.2 | async-start | bytes 2097152 | tf_op jit(solution)/shard_map/all_to_all | solution.py:66
  466.0 11.1 %copy-start.4 = (bf16[2048]{0:T(1024)(128)(2,1)S(1)}, bf16[2048]{0:T(1024)(128)(2,1)}, u32[]{:S(2)}) copy-start(bf16[2048]{0:T(1024)(128)(2,1)} %param.19) | copy-start | bytes 12292
  470.4 21.6 %all-to-all-start.4 = ((bf16[8,32,2048]{2,1,0:T(8,128)(2,1)}), bf16[8,32,2048]{2,1,0:T(8,128)(2,1)S(1)}, u32[]{:S(2)}, u32[]{:S(2)}) async-start(bf16[8,32,2048]{2,1,0:T(8,128)(2,1)} %bitcast.43), calls=%async_computation.4 | async-start | bytes 2097152 | tf_op jit(solution)/shard_map/all_to_all | solution.py:66
Sparse Core Ops, SparseCore 0:
  47.2 178.4 all-gather.10
  227.8 153.6 all-gather.12
